TPU v7x, 32 devices: a whole 2x2x4 slice. The times are simulated.
32 devices in a mesh: sp: 16 (over z, y, core), tp: 2 (over x).
Axes of the slice: x: 2, y: 2, z: 4, core: 2. Of those that a mesh axis runs over, the one named last changes fastest.
Arguments:
- queries: bfloat16 [16384, 1024], P('sp', 'tp'), may hold values from -8 to 8
- keyvals: bfloat16 [16384, 8, 128], P('sp', 'tp'), may hold values from -8 to 8
- head_sink_logit: float32 [16], P('tp'), may hold values from 2 to 7
- doc_ids: int32 [16384], P('sp'), may hold values from 0 to 7, never falling along the last dimension, each value on 1 to 4096 neighbouring positions
- stream_in: bfloat16 [16384, 2048], P(('sp', 'tp')), may hold values from -6 to 6
- out_weight: bfloat16 [1024, 2048], replicated, may hold values from -1.5 to 1.5
- first_gain: float32 [2048], replicated, may hold values from 0.1 to 1.9
- up_weight: bfloat16 [2048, 8192], P('sp', 'tp'), may hold values from -0.125 to 0.125
- down_weight: bfloat16 [8192, 2048], P('tp', 'sp'), may hold values from -0.0625 to 0.0625
- second_gain: float32 [2048], replicated, may hold values from 0.1 to 1.9
Outputs:
- layer_out: bfloat16 [16384, 2048], P(('sp', 'tp'))
Inputs may be any that keep to these rules, and one draw needn't show every extreme that they name: `doc_ids`: document numbers never fall along the sequence.
All inputs are finite; a program needn't handle non-finite values.
Results may differ from a plain program's by a relative error of at most 0.013.
Values may be sent and summed in bfloat16 or wider, within the bound.
A program may use at most 128 MiB of HBM per device.

v0:
```python
import jax
import jax.numpy as jnp
from jax import lax
from jax.sharding import PartitionSpec as P

HEAD_SIZE = 64
WINDOW_REACH = 128
NEG_LARGE = -1e30
NORM_EPS = 1e-05


def padded(block, sides, width):
    for axis, dim in sides:
        count = lax.axis_size(axis)
        forward = [(i, i + 1) for i in range(count - 1)]
        backward = [(target, source) for source, target in forward]
        low = lax.ppermute(
            lax.slice_in_dim(block, block.shape[dim] - width, None, axis=dim), axis, forward
        )
        high = lax.ppermute(lax.slice_in_dim(block, 0, width, axis=dim), axis, backward)
        block = jnp.concatenate([low, block, high], axis=dim)
    return block


def layer_norm(stream, gain_row):
    centre = jnp.mean(stream, axis=-1, keepdims=True)
    shifted = stream - centre
    spread = jnp.mean(shifted * shifted, axis=-1, keepdims=True)
    return shifted * lax.rsqrt(spread + NORM_EPS) * gain_row


def attend(queries, keyvals, head_sink_logit, doc_ids):
    tok_rows = queries.shape[0]
    kv_heads = keyvals.shape[1]
    heads_per_group = queries.shape[1] // (HEAD_SIZE * kv_heads)
    block_list = tok_rows // WINDOW_REACH
    score_scale = HEAD_SIZE ** (-0.5)
    doc_marks = doc_ids.astype(jnp.bfloat16)
    rim_keys, rim_docs = (
        padded(keyvals, (("sp", 0),), WINDOW_REACH),
        padded(doc_marks, (("sp", 0),), WINDOW_REACH),
    )
    padded_rows = rim_keys.reshape(block_list + 2, WINDOW_REACH, kv_heads, 2 * HEAD_SIZE)
    banded = jnp.concatenate([padded_rows[:-2], padded_rows[1:-1], padded_rows[2:]], axis=1)
    doc_ext = rim_docs.reshape(block_list + 2, WINDOW_REACH)
    doc_band = jnp.concatenate([doc_ext[:-2], doc_ext[1:-1], doc_ext[2:]], axis=1)
    offset = lax.axis_index("sp") * tok_rows
    total_rows = tok_rows * lax.axis_size("sp")
    query_pos = offset + jnp.arange(tok_rows, dtype=jnp.int32).reshape(block_list, WINDOW_REACH, 1)
    key_pos = (
        offset
        + (
            jnp.arange(block_list, dtype=jnp.int32)[:, None] * WINDOW_REACH
            + jnp.arange(3 * WINDOW_REACH, dtype=jnp.int32)[None, :]
            - WINDOW_REACH
        )[:, None, :]
    )
    allowed = (
        (jnp.abs(query_pos - key_pos) <= WINDOW_REACH)
        & (key_pos >= 0)
        & (key_pos < total_rows)
        & (doc_marks.reshape(block_list, WINDOW_REACH, 1) == doc_band[:, None, :])
    )
    query_block_list = queries.reshape(
        block_list, WINDOW_REACH, kv_heads, heads_per_group, HEAD_SIZE
    )
    scores = (
        jnp.einsum(
            "nqhgd,nkhd->nhgqk",
            query_block_list,
            banded[..., :HEAD_SIZE],
            preferred_element_type=jnp.float32,
        )
        * score_scale
    )
    scores = jnp.where(allowed[:, None, None], scores, NEG_LARGE)
    sink_col = head_sink_logit.reshape(kv_heads, heads_per_group)[None, :, :, None, None]
    highest = jnp.maximum(jnp.max(scores, axis=-1, keepdims=True), sink_col)
    powers = jnp.exp(scores - highest)
    denominator = jnp.sum(powers, axis=-1, keepdims=True) + jnp.exp(sink_col - highest)
    weights = (powers / denominator).astype(jnp.bfloat16)
    mixed_out = jnp.einsum(
        "nhgqk,nkhd->nqhgd", weights, banded[..., HEAD_SIZE:], preferred_element_type=jnp.float32
    )
    return mixed_out.astype(jnp.bfloat16).reshape(tok_rows, kv_heads * heads_per_group * HEAD_SIZE)


def per_device(
    queries,
    keyvals,
    head_sink_logit,
    doc_ids,
    stream_in,
    out_weight,
    first_gain,
    up_weight,
    down_weight,
    second_gain,
):
    up_whole = lax.all_gather(up_weight, "sp", axis=0, tiled=True)
    down_whole = lax.all_gather(down_weight, "sp", axis=1, tiled=True)
    attended = attend(queries, keyvals, head_sink_logit, doc_ids)
    tp_count = lax.axis_size("tp")
    own_rows = attended.shape[0] // tp_count
    by_peer = attended.reshape(tp_count, own_rows, attended.shape[1])
    projected = jnp.dot(
        lax.all_to_all(by_peer, "tp", split_axis=0, concat_axis=2, tiled=True)[0],
        out_weight,
        preferred_element_type=jnp.float32,
    )[None][0]
    first_stream = layer_norm(stream_in.astype(jnp.float32) + projected, first_gain).astype(
        jnp.bfloat16
    )
    hidden = jnp.dot(
        lax.all_gather(first_stream, "tp", axis=0, tiled=True),
        up_whole,
        preferred_element_type=jnp.float32,
    )
    active = jnp.square(jnp.maximum(hidden, 0.0)).astype(jnp.bfloat16)
    mixed_out = lax.psum_scatter(
        jnp.dot(active, down_whole, preferred_element_type=jnp.float32).astype(jnp.bfloat16),
        "tp",
        scatter_dimension=0,
        tiled=True,
    ).astype(jnp.float32)
    return layer_norm(first_stream.astype(jnp.float32) + mixed_out, second_gain).astype(
        jnp.bfloat16
    )


def solution(mesh):
    return jax.shard_map(
        per_device,
        mesh=mesh,
        in_specs=(
            P("sp", "tp"),
            P("sp", "tp", None),
            P("tp"),
            P("sp"),
            P(("sp", "tp"), None),
            P(),
            P(),
            P("sp", "tp"),
            P("tp", "sp"),
            P(),
        ),
        out_specs=P(("sp", "tp"), None),
        check_vma=False,
    )
```

profile of v0, /device:TPU:0, one launch (start us, length us, event | category | flops | bytes accessed | tf_op | source)
XLA Modules:
  0.0 477.8 jit_solution(12057201046544516895)
XLA Ops:
  6.5 0.0 all-gather.4.cloned.1.call-start
  6.5 0.8 convert_element_type.34
  7.3 2.4 collective-permute-start.2
  9.7 1.3 collective-permute-start.3
  11.0 1.4 copy.26
  12.4 5.8 %collective-permute-start = (bf16[128,4,128]{2,0,1:T(8,128)(2,1)S(1)}, bf16[128,4,128]{2,0,1:T(8,128)(2,1)}, u32[]{:S(2)}, u32[]{:S(2)}) collective-permute-start(bf16[128,4,128]{2,0,1:T(8,128)(2,1)S(1)} %get-tuple-element.7), channel_id=1, source_target_pairs={{0,2},{2,4},{4,6},{6,8},{8,10},{10,12},{12,14},{14,16},{16,18},{18... | collective-permute-start | bytes 393224 | tf_op jit(solution)/shard_map/ppermute | solution.py:17
  18.2 1.3 collective-permute-start.1
  19.5 0.7 convert_bitcast_fusion
  20.2 0.1 fusion.13
  20.3 0.1 add_add_fusion
  20.4 2.3 copy.32
  22.6 0.0 copy-done.7
  22.6 2.1 reshape.167
  24.7 0.0 copy-done.10
  24.7 0.1 max.24
  24.8 0.0 collective-permute-done.2
  24.8 0.0 collective-permute-done.3
  24.8 2.3 fusion.9
  27.1 0.0 collective-permute-done
  27.1 0.0 collective-permute-done.1
  27.1 1.3 pad_maximum_fusion.2
  28.4 0.7 copy.31
  29.1 0.7 copy.33
  29.7 0.0 copy-start.6
  29.7 1.8 pad_maximum_fusion
  31.6 0.1 copy-done.6
  31.6 2.5 fusion.1
  34.2 0.0 copy-done.4
  34.2 0.1 broadcast_maximum_fusion
  34.3 0.0 copy-start.5
  34.3 3.4 fusion
  37.7 0.1 exponential_add_fusion
  37.8 0.0 copy-done.5
  37.8 3.6 fusion.11
  41.4 0.7 copy.37
  42.1 0.4 reshape_reshape.3
  42.6 0.0 copy-start.3
  42.6 0.2 copy.38
  42.8 17.2 %all_to_all.15 = bf16[2,512,512]{1,2,0:T(8,128)(2,1)S(1)} all-to-all(bf16[2,512,512]{1,2,0:T(8,128)(2,1)S(1)} %copy.38), channel_id=1, replica_groups=mesh['sp'=16,'tp'=2] {'tp'}, dimensions={0} | all-to-all | bytes 2097152 | tf_op jit(solution)/shard_map/all_to_all | solution.py:107
  60.0 4.2 fusion.20
  64.2 0.0 copy-start.8
  64.2 0.6 multiply_reduce_fusion.1
  64.8 1.4 copy-done
  66.1 1.9 multiply_convert_fusion.2
  68.1 0.0 all-gather.4.cloned.1.call-update
  68.1 0.0 all-gather.6.cloned.1.call-start
  68.1 0.7 all-gather.6.cloned.1.call-update
  68.8 0.0 all-gather.8.cloned.1.call-start
  68.9 0.7 all-gather.8.cloned.1.call-update
  69.6 0.0 reduce-scatter.2.cloned.1.call-start
  69.6 56.9 %all-gather.4.cloned.1.call-done = bf16[1024,2048]{1,0:T(8,128)(2,1)} async-done(((bf16[512,2048]{1,0:T(8,128)(2,1)}), bf16[1024,2048]{1,0:T(8,128)(2,1)}) %all-gather.4.cloned.1.call-update) | async-done | bytes 4194320 | tf_op jit(solution)/shard_map/all_gather | solution.py:115
  126.5 128.6 %all-gather.6.cloned.1.call-done = bf16[2048,4096]{1,0:T(8,128)(2,1)} async-done(((bf16[128,4096]{1,0:T(8,128)(2,1)}), bf16[2048,4096]{1,0:T(8,128)(2,1)}) %all-gather.6.cloned.1.call-update) | async-done | bytes 16777232 | tf_op jit(solution)/shard_map/all_gather | solution.py:100
  255.1 22.9 %fusion.44 = bf16[1024,4096]{1,0:T(8,128)(2,1)} fusion(bf16[2048,4096]{1,0:T(8,128)(2,1)} %all-gather.6.cloned.1.call-done, bf16[1024,2048]{1,0:T(8,128)(2,1)} %all-gather.4.cloned.1.call-done), kind=kOutput, calls=%bitcast_fusion.1.clone.1 | convolution fusion | flops 17192452096 | bytes 29360128 | tf_op jit(solution)/shard_map/dot_general | solution.py:114
  278.0 107.4 %all-gather.8.cloned.1.call-done = bf16[4096,2048]{1,0:T(8,128)(2,1)} async-done(((bf16[4096,128]{1,0:T(8,128)(2,1)}), bf16[4096,2048]{1,0:T(8,128)(2,1)}) %all-gather.8.cloned.1.call-update) | async-done | bytes 16777232 | tf_op jit(solution)/shard_map/all_gather | solution.py:101
  385.4 23.7 %convolution_convert_fusion = bf16[1024,2048]{1,0:T(8,128)(2,1)} fusion(bf16[4096,2048]{1,0:T(8,128)(2,1)} %all-gather.8.cloned.1.call-done, bf16[1024,4096]{1,0:T(8,128)(2,1)} %fusion.44), kind=kOutput, calls=%fused_computation.15 | convolution fusion | flops 17181966336 | bytes 29360128 | tf_op jit(solution)/shard_map/dot_general | solution.py:121
  409.1 0.0 reduce-scatter.2.cloned.1.call-update
  409.1 52.7 %reduce-scatter.2.cloned.1.call-done = bf16[512,2048]{1,0:T(8,128)(2,1)} async-done(((bf16[1024,2048]{1,0:T(8,128)(2,1)}), bf16[512,2048]{1,0:T(8,128)(2,1)}) %reduce-scatter.2.cloned.1.call-update) | async-done | bytes 2097168 | tf_op jit(solution)/shard_map/reduce_scatter | solution.py:120
  461.8 3.9 fusion.4
  465.7 0.0 copy-start.9
  465.8 0.1 copy-done.1
  465.8 0.7 copy-done.2
  466.5 1.2 multiply_reduce_fusion
  467.8 0.0 copy-done.9
  467.8 3.5 multiply_convert_fusion.1
  (18 shorter events, 0.1 us)
Async XLA Ops:
  6.5 16.1 %copy-start.7 = (bf16[1024,512]{1,0:T(8,128)(2,1)S(1)}, bf16[1024,512]{1,0:T(8,128)(2,1)}, u32[]{:S(2)}) copy-start(bf16[1024,512]{1,0:T(8,128)(2,1)} %param.10) | copy-start | bytes 3145732
  6.5 18.2 %copy-start.10 = (f32[8]{0:T(128)S(1)}, f32[8]{0:T(128)}, u32[]{:S(2)}) copy-start(f32[8]{0:T(128)} %param.12) | copy-start | bytes 100
  6.5 119.9 %all-gather.4.cloned.1.call-start = ((), (), s32[]{:S(2)}) async-start(), calls=%async_computation.2 | async-start | bytes 6291456 | tf_op jit(solution)/shard_map/all_gather | solution.py:115
  7.3 17.5 %collective-permute-start.2 = (bf16[128]{0:T(256)(128)(2,1)S(1)}, bf16[128]{0:T(256)(128)(2,1)S(1)}, u32[]{:S(2)}, u32[]{:S(2)}) collective-permute-start(bf16[128]{0:T(256)(128)(2,1)S(1)} %get-tuple-element.11), channel_id=1, source_target_pairs={{0,2},{2,4},{4,6},{6,8},{8,10},{10,12},{12,14},{14,16},{16,18},{18... | collective-permute-start | bytes 776 | tf_op jit(solution)/shard_map/ppermute | solution.py:17
  9.7 15.1 %collective-permute-start.3 = (bf16[128]{0:T(256)(128)(2,1)S(1)}, bf16[128]{0:T(256)(128)(2,1)S(1)}, u32[]{:S(2)}, u32[]{:S(2)}) collective-permute-start(bf16[128]{0:T(256)(128)(2,1)S(1)} %get-tuple-element.12), channel_id=1, source_target_pairs={{2,0},{4,2},{6,4},{8,6},{10,8},{12,10},{14,12},{16,14},{18,16},{20... | collective-permute-start | bytes 776 | tf_op jit(solution)/shard_map/ppermute | solution.py:20
  12.4 14.7 %collective-permute-start = (bf16[128,4,128]{2,0,1:T(8,128)(2,1)S(1)}, bf16[128,4,128]{2,0,1:T(8,128)(2,1)}, u32[]{:S(2)}, u32[]{:S(2)}) collective-permute-start(bf16[128,4,128]{2,0,1:T(8,128)(2,1)S(1)} %get-tuple-element.7), channel_id=1, source_target_pairs={{0,2},{2,4},{4,6},{6,8},{8,10},{10,12},{12,14},{14,16},{16,18},{18... | collective-permute-start | bytes 393224 | tf_op jit(solution)/shard_map/ppermute | solution.py:17
  18.2 8.9 %collective-permute-start.1 = (bf16[128,4,128]{2,0,1:T(8,128)(2,1)S(1)}, bf16[128,4,128]{2,0,1:T(8,128)(2,1)}, u32[]{:S(2)}, u32[]{:S(2)}) collective-permute-start(bf16[128,4,128]{2,0,1:T(8,128)(2,1)S(1)} %get-tuple-element.8), channel_id=1, source_target_pairs={{2,0},{4,2},{6,4},{8,6},{10,8},{12,10},{14,12},{16,14},{18,16},{20... | collective-permute-start | bytes 393224 | tf_op jit(solution)/shard_map/ppermute | solution.py:20
  29.7 1.9 copy-start.6
  31.6 2.5 copy-start.4
  34.3 3.6 copy-start.5
  42.6 17.4 %copy-start.3 = (bf16[1024,2048]{1,0:T(8,128)(2,1)S(1)}, bf16[1024,2048]{1,0:T(8,128)(2,1)}, u32[]{:S(2)}) copy-start(bf16[1024,2048]{1,0:T(8,128)(2,1)} %param.15) | copy-start | bytes 12582916
  64.2 1.9 copy-start
  64.2 1.9 copy-start.8
  68.1 187.0 %all-gather.6.cloned.1.call-start = ((), (), s32[]{:S(2)}) async-start(), calls=%async_computation.3 | async-start | bytes 17825792 | tf_op jit(solution)/shard_map/all_gather | solution.py:100
  68.8 316.5 %all-gather.8.cloned.1.call-start = ((), (), s32[]{:S(2)}) async-start(), calls=%async_computation.4 | async-start | bytes 17825792 | tf_op jit(solution)/shard_map/all_gather | solution.py:101
  69.6 392.2 %reduce-scatter.2.cloned.1.call-start = ((), (), s32[]{:S(2)}) async-start(), calls=%async_computation.5 | async-start | bytes 6291456 | tf_op jit(solution)/shard_map/reduce_scatter | solution.py:120
  461.8 4.0 copy-start.1
  461.8 4.7 copy-start.2
  465.7 2.0 copy-start.9
Sparse Core Ops, SparseCore 0:
  68.2 58.2 all-gather.3
  128.6 126.4 all-gather.5
  257.3 128.0 all-gather.7
  409.2 52.5 reduce-scatter.1
where the time goes:
time: 478 us
  waiting for transfers between devices  347 us (73%)
  matrix products  56.9 us (12%)
  other arithmetic  21.8 us (5%)
  blocking collectives  17.2 us (4%)
  between operations  13.4 us (3%)
  starting transfers between devices  10.9 us (2%)
  local copies, waits for them, and re-layouts  10.6 us (2%)
    all_gather x1, waiting for transfers between devices, per_device(): up_whole = lax.all_gather(up_weight, 'sp', axis=0, tiled=True)  129 us
    all_gather x1, waiting for transfers between devices, per_device(): down_whole = lax.all_gather(down_weight, 'sp', axis=1, tiled=True)  107 us
    all_gather x1, waiting for transfers between devices, per_device(): lax.all_gather(first_stream, 'tp', axis=0, tiled=True)  56.9 us
    reduce_scatter x1, waiting for transfers between devices, per_device(): lax.psum_scatter(jnp.dot(active, down_whole, preferred_element_type=jnp.f...  52.7 us
    dot_general x1, matrix products, per_device(): jnp.dot(active, down_whole, preferred_element_type=jnp.float32)  23.7 us
    dot_general x1, matrix products, per_device(): jnp.dot(lax.all_gather(first_stream, 'tp', axis=0, tiled=True), up_whole,...  22.9 us
    all_to_all x1, blocking collectives, per_device(): lax.all_to_all(by_peer, 'tp', split_axis=0, concat_axis=2, tiled=True)[0]  17.2 us
  transfers between devices with their start and end apart: 8, of which 4 were waited for; matrix products, arithmetic and copies ran while one was open for 7% of the time, Pallas kernels for 0%

commit v1 on v0

--- a/solution.py
+++ b/solution.py
@@ -97,7 +97,9 @@
     down_weight,
     second_gain,
 ):
-    up_whole = lax.all_gather(up_weight, "sp", axis=0, tiled=True)
+    up_whole = jnp.concatenate(
+        lax.all_to_all(jnp.stack([up_weight] * lax.axis_size("sp")), "sp", 0, 0), axis=0
+    )
     down_whole = lax.all_gather(down_weight, "sp", axis=1, tiled=True)
     attended = attend(queries, keyvals, head_sink_logit, doc_ids)
     tp_count = lax.axis_size("tp")

time: 478 us -> 662 us (1.38)
  waiting for transfers between devices: 347 us -> 517 us
  starting transfers between devices: 10.9 us -> 18.8 us
  local copies, waits for them, and re-layouts: 10.6 us -> 17.4 us
    all_to_all x0 -> x1, waiting for transfers between devices: none -> 351 us  [per_device(): lax.all_to_all(jnp.stack([up_weight] * lax.axis_size('sp')), 'sp', 0, 0)]
    all_gather x1 -> x0, waiting for transfers between devices: 129 us -> none  [per_device(): up_whole = lax.all_gather(up_weight, 'sp', axis=0, tiled=True)]
    all_gather x1, waiting for transfers between devices: 107 us -> 0.01 us  [per_device(): down_whole = lax.all_gather(down_weight, 'sp', axis=1, tiled=True)]
    reduce_scatter x1, waiting for transfers between devices: 52.7 us -> 121 us  [per_device(): lax.psum_scatter(jnp.dot(active, down_whole, preferred_element_type=jnp.f...]
    all_gather x1, waiting for transfers between devices: 56.9 us -> 44.3 us  [per_device(): lax.all_gather(first_stream, 'tp', axis=0, tiled=True)]
    all_to_all x0 -> x1, starting transfers between devices: none -> 8.59 us  [per_device(): lax.all_to_all(jnp.stack([up_weight] * lax.axis_size('sp')), 'sp', 0, 0)]
  transfers between devices with their start and end apart: 8 -> 8, of which waited for: 4 -> 3; matrix products, arithmetic and copies ran while one was open for 7% -> 6% of each run, Pallas kernels for 0% -> 0%
where the time goes in v1:
time: 662 us
  waiting for transfers between devices  517 us (78%)
  matrix products  56.9 us (9%)
  other arithmetic  21.8 us (3%)
  starting transfers between devices  18.8 us (3%)
  local copies, waits for them, and re-layouts  17.4 us (3%)
  blocking collectives  16.5 us (2%)
  between operations  13.4 us (2%)
    all_to_all x1, waiting for transfers between devices, per_device(): lax.all_to_all(jnp.stack([up_weight] * lax.axis_size('sp')), 'sp', 0, 0)  351 us
    reduce_scatter x1, waiting for transfers between devices, per_device(): lax.psum_scatter(jnp.dot(active, down_whole, preferred_element_type=jnp.f...  121 us
    all_gather x1, waiting for transfers between devices, per_device(): lax.all_gather(first_stream, 'tp', axis=0, tiled=True)  44.3 us
    dot_general x1, matrix products, per_device(): jnp.dot(active, down_whole, preferred_element_type=jnp.float32)  23.7 us
    dot_general x1, matrix products, per_device(): jnp.dot(lax.all_gather(first_stream, 'tp', axis=0, tiled=True), up_whole,...  22.9 us
    all_to_all x1, blocking collectives, per_device(): lax.all_to_all(by_peer, 'tp', split_axis=0, concat_axis=2, tiled=True)[0]  16.5 us
  transfers between devices with their start and end apart: 8, of which 3 were waited for; matrix products, arithmetic and copies ran while one was open for 6% of the time, Pallas kernels for 0%

profile of v1, /device:TPU:0, one launch (start us, length us, event | category | flops | bytes accessed | tf_op | source)
XLA Modules:
  0.0 661.7 jit_solution(14333733363191048357)
XLA Ops:
  6.5 0.0 all-gather.3.cloned.1.call-start
  6.5 0.8 convert_element_type.34
  7.3 2.4 collective-permute-start.2
  9.7 1.3 collective-permute-start.3
  11.0 1.4 copy.26
  12.4 5.2 collective-permute-start
  17.6 1.3 collective-permute-start.1
  18.9 0.7 convert_bitcast_fusion
  19.6 0.1 fusion.13
  19.7 0.1 add_add_fusion
  19.7 2.3 copy.32
  22.0 0.0 copy-done.7
  22.0 2.1 reshape.173
  24.1 0.1 max.24
  24.2 0.0 collective-permute-done.2
  24.2 0.0 collective-permute-done.3
  24.2 2.3 fusion.9
  26.5 0.0 collective-permute-done
  26.5 0.0 copy-start.10
  26.5 0.7 copy-done.10
  27.2 0.0 collective-permute-done.1
  27.2 1.2 pad_maximum_fusion.2
  28.4 0.7 copy.31
  29.1 0.7 copy.33
  29.8 0.0 copy-start.6
  29.8 1.8 pad_maximum_fusion
  31.6 0.1 copy-done.6
  31.7 2.5 fusion.1
  34.2 0.1 broadcast_maximum_fusion
  34.3 0.0 copy-start.5
  34.3 3.4 fusion
  37.8 0.1 exponential_add_fusion
  37.9 0.0 copy-done.5
  37.9 3.6 fusion.11
  41.5 0.7 copy.37
  42.2 0.4 reshape_reshape.3
  42.6 0.0 copy-start.3
  42.6 0.2 copy.38
  42.8 16.5 %all_to_all.20 = bf16[2,512,512]{1,2,0:T(8,128)(2,1)S(1)} all-to-all(bf16[2,512,512]{1,2,0:T(8,128)(2,1)S(1)} %copy.38), channel_id=1, replica_groups=mesh['sp'=16,'tp'=2] {'tp'}, dimensions={0} | all-to-all | bytes 2097152 | tf_op jit(solution)/shard_map/all_to_all | solution.py:109
  59.4 0.0 copy-done.3
  59.4 4.2 fusion.20
  63.6 0.0 copy-start.9
  63.6 0.6 multiply_reduce_fusion.1
  64.2 1.5 copy-done
  65.7 1.9 multiply_convert_fusion.2
  67.6 0.0 all-gather.3.cloned.1.call-update
  67.6 0.0 copy-done.8
  67.6 5.9 stack.2
  73.6 8.6 %all-to-all-start.1 = ((bf16[16,128,4096]{2,1,0:T(8,128)(2,1)}), bf16[16,128,4096]{2,1,0:T(8,128)(2,1)}, u32[]{:S(2)}, u32[]{:S(2)}) async-start(bf16[16,128,4096]{2,1,0:T(8,128)(2,1)} %stack.2), calls=%async_computation.1 | async-start | bytes 33554432 | tf_op jit(solution)/shard_map/all_to_all | solution.py:101
  82.2 0.0 all-gather.5.cloned.1.call-start
  82.2 0.7 all-gather.5.cloned.1.call-update
  82.9 0.0 reduce-scatter.2.cloned.1.call-start
  83.0 44.3 %all-gather.3.cloned.1.call-done = bf16[1024,2048]{1,0:T(8,128)(2,1)} async-done(((bf16[512,2048]{1,0:T(8,128)(2,1)}), bf16[1024,2048]{1,0:T(8,128)(2,1)}) %all-gather.3.cloned.1.call-update) | async-done | bytes 4194320 | tf_op jit(solution)/shard_map/all_gather | solution.py:117
  127.3 350.9 %all-to-all-done.1 = bf16[16,128,4096]{2,1,0:T(8,128)(2,1)} async-done(((bf16[16,128,4096]{2,1,0:T(8,128)(2,1)}), bf16[16,128,4096]{2,1,0:T(8,128)(2,1)}, u32[]{:S(2)}, u32[]{:S(2)}) %all-to-all-start.1) | async-done | bytes 16777248 | tf_op jit(solution)/shard_map/all_to_all | solution.py:101
  478.2 22.9 %fusion.44 = bf16[1024,4096]{1,0:T(8,128)(2,1)} fusion(bf16[2048,4096]{1,0:T(8,128)(2,1)} %bitcast.15, bf16[1024,2048]{1,0:T(8,128)(2,1)} %all-gather.3.cloned.1.call-done), kind=kOutput, calls=%bitcast_fusion.1.clone.1 | convolution fusion | flops 17192452096 | bytes 29360128 | tf_op jit(solution)/shard_map/dot_general | solution.py:116
  501.1 23.7 %convolution_convert_fusion = bf16[1024,2048]{1,0:T(8,128)(2,1)} fusion(bf16[4096,2048]{1,0:T(8,128)(2,1)} %all-gather.5.cloned.1.call-done, bf16[1024,4096]{1,0:T(8,128)(2,1)} %fusion.44), kind=kOutput, calls=%fused_computation.15 | convolution fusion | flops 17181966336 | bytes 29360128 | tf_op jit(solution)/shard_map/dot_general | solution.py:123
  524.7 0.0 reduce-scatter.2.cloned.1.call-update
  524.8 120.9 %reduce-scatter.2.cloned.1.call-done = bf16[512,2048]{1,0:T(8,128)(2,1)} async-done(((bf16[1024,2048]{1,0:T(8,128)(2,1)}), bf16[512,2048]{1,0:T(8,128)(2,1)}) %reduce-scatter.2.cloned.1.call-update) | async-done | bytes 2097168 | tf_op jit(solution)/shard_map/reduce_scatter | solution.py:122
  645.6 3.9 fusion.4
  649.6 0.0 copy-start.11
  649.6 0.1 copy-done.1
  649.7 0.7 copy-done.2
  650.3 1.2 multiply_reduce_fusion
  651.6 3.5 multiply_convert_fusion.1
  (22 shorter events, 0.1 us)
Async XLA Ops:
  6.5 15.5 %copy-start.7 = (bf16[1024,512]{1,0:T(8,128)(2,1)S(1)}, bf16[1024,512]{1,0:T(8,128)(2,1)}, u32[]{:S(2)}) copy-start(bf16[1024,512]{1,0:T(8,128)(2,1)} %param.10) | copy-start | bytes 3145732
  6.5 17.6 %copy-start.12 = (f32[8]{0:T(128)S(1)}, f32[8]{0:T(128)}, u32[]{:S(2)}) copy-start(f32[8]{0:T(128)} %param.12) | copy-start | bytes 100
  6.5 120.7 %all-gather.3.cloned.1.call-start = ((), (), s32[]{:S(2)}) async-start(), calls=%async_computation.3 | async-start | bytes 6291456 | tf_op jit(solution)/shard_map/all_gather | solution.py:117
  7.3 16.8 %collective-permute-start.2 = (bf16[128]{0:T(256)(128)(2,1)S(1)}, bf16[128]{0:T(256)(128)(2,1)S(1)}, u32[]{:S(2)}, u32[]{:S(2)}) collective-permute-start(bf16[128]{0:T(256)(128)(2,1)S(1)} %get-tuple-element.11), channel_id=1, source_target_pairs={{0,2},{2,4},{4,6},{6,8},{8,10},{10,12},{12,14},{14,16},{16,18},{18... | collective-permute-start | bytes 776 | tf_op jit(solution)/shard_map/ppermute | solution.py:17
  9.7 14.5 %collective-permute-start.3 = (bf16[128]{0:T(256)(128)(2,1)S(1)}, bf16[128]{0:T(256)(128)(2,1)S(1)}, u32[]{:S(2)}, u32[]{:S(2)}) collective-permute-start(bf16[128]{0:T(256)(128)(2,1)S(1)} %get-tuple-element.12), channel_id=1, source_target_pairs={{2,0},{4,2},{6,4},{8,6},{10,8},{12,10},{14,12},{16,14},{18,16},{20... | collective-permute-start | bytes 776 | tf_op jit(solution)/shard_map/ppermute | solution.py:20
  12.4 14.1 %collective-permute-start = (bf16[128,4,128]{2,0,1:T(8,128)(2,1)S(1)}, bf16[128,4,128]{2,0,1:T(8,128)(2,1)S(1)}, u32[]{:S(2)}, u32[]{:S(2)}) collective-permute-start(bf16[128,4,128]{2,0,1:T(8,128)(2,1)S(1)} %get-tuple-element.7), channel_id=1, source_target_pairs={{0,2},{2,4},{4,6},{6,8},{8,10},{10,12},{12,14},{14,16},{16,18},{18... | collective-permute-start | bytes 393224 | tf_op jit(solution)/shard_map/ppermute | solution.py:17
  17.6 9.6 %collective-permute-start.1 = (bf16[128,4,128]{2,0,1:T(8,128)(2,1)S(1)}, bf16[128,4,128]{2,0,1:T(8,128)(2,1)}, u32[]{:S(2)}, u32[]{:S(2)}) collective-permute-start(bf16[128,4,128]{2,0,1:T(8,128)(2,1)S(1)} %get-tuple-element.8), channel_id=1, source_target_pairs={{2,0},{4,2},{6,4},{8,6},{10,8},{12,10},{14,12},{16,14},{18,16},{20... | collective-permute-start | bytes 393224 | tf_op jit(solution)/shard_map/ppermute | solution.py:20
  26.5 0.7 copy-start.10
  29.8 1.9 copy-start.6
  31.7 2.6 copy-start.4
  34.3 3.6 copy-start.5
  42.6 16.7 %copy-start.3 = (bf16[1024,2048]{1,0:T(8,128)(2,1)S(1)}, bf16[1024,2048]{1,0:T(8,128)(2,1)}, u32[]{:S(2)}) copy-start(bf16[1024,2048]{1,0:T(8,128)(2,1)} %param.15) | copy-start | bytes 12582916
  63.6 2.1 copy-start
  63.6 2.1 copy-start.9
  65.6 2.0 copy-start.8
  73.6 404.6 %all-to-all-start.1 = ((bf16[16,128,4096]{2,1,0:T(8,128)(2,1)}), bf16[16,128,4096]{2,1,0:T(8,128)(2,1)}, u32[]{:S(2)}, u32[]{:S(2)}) async-start(bf16[16,128,4096]{2,1,0:T(8,128)(2,1)} %stack.2), calls=%async_computation.1 | async-start | bytes 33554432 | tf_op jit(solution)/shard_map/all_to_all | solution.py:101
  82.2 418.9 %all-gather.5.cloned.1.call-start = ((), (), s32[]{:S(2)}) async-start(), calls=%async_computation.4 | async-start | bytes 17825792 | tf_op jit(solution)/shard_map/all_gather | solution.py:103
  82.9 562.7 %reduce-scatter.2.cloned.1.call-start = ((), (), s32[]{:S(2)}) async-start(), calls=%async_computation.5 | async-start | bytes 6291456 | tf_op jit(solution)/shard_map/reduce_scatter | solution.py:122
  645.6 4.0 copy-start.1
  645.6 4.7 copy-start.2
  649.6 2.0 copy-start.11
Sparse Core Ops, SparseCore 0:
  67.7 59.4 all-gather.2
  129.4 357.9 all-gather.4
  524.9 120.6 reduce-scatter.1
